TPU v7x, 32 devices: a whole 2x2x4 slice. The times are simulated.
32 devices in a mesh: ep: 8 (over z, x), tp: 4 (over y, core).
Axes of the slice: x: 2, y: 2, z: 4, core: 2. Of those that a mesh axis runs over, the one named last changes fastest.
Arguments:
- queries: bfloat16 [2048, 2048], P('ep', 'tp'), may hold values from -9 to 9
- keys: bfloat16 [2048, 2048], P('ep', 'tp'), may hold values from -9 to 9
- values: bfloat16 [2048, 2048], P('ep', 'tp'), may hold values from -6 to 6
- lambdas: float32 [16], P('tp'), may hold values from 0.3 to 0.8
- head_gain: float32 [128], replicated, may hold values from 0.1 to 1.9
- moe_input: bfloat16 [4096, 2048], P('ep'), may hold values from -6 to 6
- ffn_gain: float32 [2048], replicated, may hold values from 0.1 to 1.9
- group_router: bfloat16 [2048, 4], replicated, may hold values from -0.125 to 0.125
- expert_router: bfloat16 [2048, 8], replicated, may hold values from -0.125 to 0.125
- routes: int32 [4096, 2], P('ep'), may hold values from 0 to 7, as said below
- w_gate: bfloat16 [8, 2048, 1024], P('ep', None, 'tp'), may hold values from -0.125 to 0.125
- w_up: bfloat16 [8, 2048, 1024], P('ep', None, 'tp'), may hold values from -0.125 to 0.125
- w_down: bfloat16 [8, 1024, 2048], P('ep', 'tp'), may hold values from -0.1875 to 0.1875
Outputs:
- attn_out: bfloat16 [2048, 2048], P('ep', 'tp')
- moe_out: bfloat16 [4096, 2048], P(('ep', 'tp'))
Inputs may be any that keep to these rules, and one draw needn't show every extreme that they name: `routes`: in each aligned block of 128 rows (the rows of one device) every expert is named by exactly 32 rows and every group by the same number of rows; a row's two experts differ and lie in one group of 2 consecutive expert numbers.
All inputs are finite; a program needn't handle non-finite values.
Results may differ from a plain program's by a relative error of at most 0.015.
Values may be sent and summed in bfloat16 or wider, within the bound.
A program may use at most 128 MiB of HBM per device.

v0:
```python
import math
import jax
import jax.numpy as jnp
from jax import lax
from jax.sharding import PartitionSpec as P

norm_eps = 1e-06
masked_score = -1e30


def rms_scaled(rows, gain):
    widened = rows.astype(jnp.float32)
    return (
        widened * lax.rsqrt(jnp.mean(widened * widened, axis=-1, keepdims=True) + norm_eps) * gain
    )


def score_block(query_heads, key_rows, score_scale):
    key_heads = key_rows.reshape(key_rows.shape[0], query_heads.shape[1], 2, query_heads.shape[3])
    return (
        jnp.einsum("qhmd,khmd->hmqk", query_heads, key_heads, preferred_element_type=jnp.float32)
        * score_scale
    )


def route_gates(normed, own_routes, group_router, expert_router):
    group_count = group_router.shape[1]
    expert_count = expert_router.shape[1]
    group_logits = jnp.dot(normed, group_router, preferred_element_type=jnp.float32)
    expert_logits = jnp.dot(normed, expert_router, preferred_element_type=jnp.float32)
    chosen = own_routes[:, 0] // (expert_count // group_count)
    group_mask = jnp.arange(group_count, dtype=jnp.int32)[None, :] == chosen[:, None]
    own_logit = jnp.sum(jnp.where(group_mask, group_logits, 0.0), axis=-1, keepdims=True)
    group_share = 1.0 / jnp.sum(jnp.exp(group_logits - own_logit), axis=-1)
    expert_mask = jnp.arange(expert_count, dtype=jnp.int32)[None, None, :] == own_routes[:, :, None]
    picked = jnp.sum(jnp.where(expert_mask, expert_logits[:, None, :], 0.0), axis=-1)
    return group_share[:, None] * jax.nn.sigmoid(picked - picked[:, ::-1])


def slot_places(own_routes, expert_count, capacity):
    flat_routes = own_routes.reshape(-1)
    one_hot = (flat_routes[:, None] == jnp.arange(expert_count, dtype=jnp.int32)[None, :]).astype(
        jnp.int32
    )
    earlier = jnp.cumsum(one_hot, axis=0) - one_hot
    return flat_routes * capacity + jnp.sum(earlier * one_hot, axis=1)


def dispatch_rows(normed_rows, own_routes, expert_count, capacity):
    places = slot_places(own_routes, expert_count, capacity)
    owners = jnp.arange(places.shape[0], dtype=jnp.int32) // 2
    holder = jnp.zeros((expert_count * capacity,), jnp.int32).at[places].set(owners)
    return normed_rows[holder].reshape(expert_count, capacity, normed_rows.shape[1])


def local(
    queries,
    keys,
    values,
    lambdas,
    head_gain,
    moe_input,
    ffn_gain,
    group_router,
    expert_router,
    routes,
    w_gate,
    w_up,
    w_down,
):
    query_count = queries.shape[0]
    heads_here = lambdas.shape[0]
    value_width = values.shape[1] // heads_here
    qk_width = queries.shape[1] // (2 * heads_here)
    query_heads = queries.reshape(query_count, heads_here, 2, qk_width)
    score_scale = qk_width ** (-0.5)
    query_first = lax.axis_index("ep") * query_count
    query_pos = query_first + jnp.arange(query_count, dtype=jnp.int32)
    query_last = query_first + query_count - 1
    stats_start = (
        jnp.full((heads_here, 2, query_count), masked_score, jnp.float32),
        jnp.zeros((heads_here, 2, query_count), jnp.float32),
    )
    key_shard = lax.all_gather(keys, "ep", axis=0, tiled=True)
    block_rows = math.gcd(key_shard.shape[0], 512)

    def stats_sweep_step(number, current):
        offset = number * block_rows

        def stats_compute(running):
            maxima, totals = running
            key_pos = offset + jnp.arange(block_rows, dtype=jnp.int32)
            allowed = key_pos[None, :] <= query_pos[:, None]
            key_block = lax.dynamic_slice_in_dim(key_shard, offset, block_rows, 0)
            scores = jnp.where(
                allowed, score_block(query_heads, key_block, score_scale), masked_score
            )
            new_max = jnp.maximum(maxima, jnp.max(scores, axis=-1))
            weights = jnp.where(allowed, jnp.exp(scores - new_max[..., None]), 0.0)
            return (new_max, totals * jnp.exp(maxima - new_max) + jnp.sum(weights, axis=-1))

        return lax.cond(offset <= query_last, stats_compute, lambda running: running, current)

    maxima, totals = lax.fori_loop(
        0, key_shard.shape[0] // block_rows, stats_sweep_step, stats_start
    )
    value_key_shard = lax.all_gather(keys, "ep", axis=0, tiled=True)
    value_shard = lax.all_gather(values, "ep", axis=0, tiled=True)
    value_block_rows = math.gcd(value_key_shard.shape[0], 512)

    def value_sweep_step(number, current):
        offset = number * value_block_rows

        def value_compute(running):
            key_pos = offset + jnp.arange(value_block_rows, dtype=jnp.int32)
            allowed = key_pos[None, :] <= query_pos[:, None]
            key_block = lax.dynamic_slice_in_dim(value_key_shard, offset, value_block_rows, 0)
            scores = score_block(query_heads, key_block, score_scale)
            shares = (
                jnp.where(allowed, jnp.exp(scores - maxima[..., None]), 0.0) / totals[..., None]
            )
            mixed = (shares[:, 0] - lambdas[:, None, None] * shares[:, 1]).astype(jnp.bfloat16)
            value_rows = lax.dynamic_slice_in_dim(value_shard, offset, value_block_rows, 0).reshape(
                value_block_rows, heads_here, value_width
            )
            return running + jnp.einsum(
                "hqk,khd->hqd", mixed, value_rows, preferred_element_type=jnp.float32
            )

        return lax.cond(offset <= query_last, value_compute, lambda running: running, current)

    heads_out = lax.fori_loop(
        0,
        value_key_shard.shape[0] // value_block_rows,
        value_sweep_step,
        jnp.zeros((heads_here, query_count, value_width), jnp.float32),
    )
    attn_out = rms_scaled(heads_out, head_gain).astype(jnp.bfloat16)
    attn_out = attn_out.transpose(1, 0, 2).reshape(query_count, heads_here * value_width)
    tp_count = lax.axis_size("tp")
    tp_index = lax.axis_index("tp")
    own_count = routes.shape[0] // tp_count
    expert_count = expert_router.shape[1]
    capacity = 2 * own_count // expert_count
    model_width = moe_input.shape[1]
    own_routes = lax.dynamic_slice_in_dim(routes, tp_index * own_count, own_count, 0)
    gate_local = w_gate[0]
    up_local = w_up[0]
    down_local = w_down[0]
    own_input = lax.dynamic_slice_in_dim(moe_input, tp_index * own_count, own_count, 0)
    normed = rms_scaled(own_input, ffn_gain).astype(jnp.bfloat16)
    packed = dispatch_rows(normed, own_routes, expert_count, capacity)
    arrived = lax.all_to_all(packed, "ep", split_axis=0, concat_axis=0, tiled=True)
    arrived_rows = lax.all_gather(arrived.reshape(-1, model_width), "tp", axis=0, tiled=True)
    gate_part = jnp.dot(arrived_rows, gate_local, preferred_element_type=jnp.float32)
    up_part = jnp.dot(arrived_rows, up_local, preferred_element_type=jnp.float32)
    hidden = (jax.nn.silu(gate_part) * up_part).astype(jnp.bfloat16)
    summed = lax.psum_scatter(
        jnp.dot(hidden, down_local, preferred_element_type=jnp.float32).astype(jnp.bfloat16),
        "tp",
        scatter_dimension=0,
        tiled=True,
    )
    homed = lax.all_to_all(
        summed.reshape(expert_count, capacity, model_width),
        "ep",
        split_axis=0,
        concat_axis=0,
        tiled=True,
    )
    places = slot_places(own_routes, expert_count, capacity)
    returned = homed.reshape(expert_count * capacity, model_width)[places].reshape(
        own_count, 2, model_width
    )
    gates = route_gates(normed, own_routes, group_router, expert_router)
    moe_out = jnp.sum(returned.astype(jnp.float32) * gates[..., None], axis=1).astype(jnp.bfloat16)
    return (attn_out, moe_out)


def solution(mesh):
    in_specs = (
        P("ep", "tp"),
        P("ep", "tp"),
        P("ep", "tp"),
        P("tp"),
        P(),
        P("ep", None),
        P(),
        P(),
        P(),
        P("ep", None),
        P("ep", None, "tp"),
        P("ep", None, "tp"),
        P("ep", "tp", None),
    )
    out_specs = (P("ep", "tp"), P(("ep", "tp"), None))
    return jax.shard_map(local, mesh=mesh, in_specs=in_specs, out_specs=out_specs, check_vma=False)
```

profile of v0, /device:TPU:25, one launch (start us, length us, event | category | flops | bytes accessed | tf_op | source)
XLA Modules:
  0.0 235.7 jit_solution(4646205072305375631)
XLA Ops:
  11.7 1.4 scatter_custom_fusion
  14.4 1.4 gather_fusion
  15.8 28.6 %all_to_all.10 = bf16[8,32,2048]{2,1,0:T(8,128)(2,1)} all-to-all(bf16[8,32,2048]{2,1,0:T(8,128)(2,1)S(1)} %bitcast.83), channel_id=1, replica_groups=mesh['ep'=8,'tp'=4] {'ep'}, dimensions={0} | all-to-all | bytes 2097152 | tf_op jit(solution)/shard_map/all_to_all | solution.py:153
  44.4 36.6 %all-gather.8.cloned.1.call-done = bf16[1024,2048]{1,0:T(8,128)(2,1)} async-done(((bf16[256,2048]{1,0:T(8,128)(2,1)}), bf16[1024,2048]{1,0:T(8,128)(2,1)}) %all-gather.8.cloned.1.call-update) | async-done | bytes 4194320 | tf_op jit(solution)/shard_map/all_gather | solution.py:154
  81.0 4.8 %fusion.18 = f32[1024,256]{1,0:T(8,128)} fusion(bf16[1024,2048]{1,0:T(8,128)(2,1)} %all-gather.8.cloned.1.call-done, bf16[1,2048,256]{2,1,0:T(8,128)(2,1)} %param.31), kind=kOutput, calls=%fused_computation.38 | convolution fusion | flops 1073741824 | bytes 6291456 | tf_op jit(solution)/shard_map/dot_general | solution.py:155
  85.9 8.8 %convolution_convert_fusion = bf16[1024,2048]{1,0:T(8,128)(2,1)} fusion(bf16[1024,2048]{1,0:T(8,128)(2,1)} %all-gather.8.cloned.1.call-done, bf16[1,256,2048]{2,1,0:T(8,128)(2,1)S(1)} %copy-done, bf16[1,2048,256]{2,1,0:T(8,128)(2,1)S(1)} %copy-done.8, f32[1024,256]{1,0:T(8,128)} %fusion.18), kind=kOutput, calls=%fused_computation.27 | convolution fusion | flops 2151153664 | bytes 11534336 | tf_op jit(solution)/shard_map/dot_general | solution.py:159
  97.8 41.1 %reduce-scatter.2.cloned.1.call-done = bf16[256,2048]{1,0:T(8,128)(2,1)} async-done(((bf16[1024,2048]{1,0:T(8,128)(2,1)}), bf16[256,2048]{1,0:T(8,128)(2,1)}) %reduce-scatter.2.cloned.1.call-update) | async-done | bytes 1048592 | tf_op jit(solution)/shard_map/reduce_scatter | solution.py:158
  138.8 5.4 %all-to-all-start.1 = ((bf16[8,32,2048]{2,1,0:T(8,128)(2,1)}), bf16[8,32,2048]{2,1,0:T(8,128)(2,1)S(1)}, u32[]{:S(2)}, u32[]{:S(2)}) async-start(bf16[8,32,2048]{2,1,0:T(8,128)(2,1)} %bitcast.86), calls=%async_computation.2 | async-start | bytes 2097152 | tf_op jit(solution)/shard_map/all_to_all | solution.py:164
  146.0 13.0 %while.33 = (s32[]{:T(128)}, f32[4,2,256]{2,1,0:T(2,128)S(1)}, f32[4,2,256]{2,1,0:T(2,128)S(1)}, s32[]{:T(128)}, bf16[2048,512]{0,1:T(8,128)(2,1)}, /*index=5*/b...) while((s32[]{:T(128)}, f32[4,2,256]{2,1,0:T(2,128)S(1)}, ...), condition=%wide.region_5.6_spmd.clone, body=%wide.region_0.5_spmd.clone.sunk | while | flops 142742272 | bytes 10731789 | solution.py:104
  146.0 3.2 %conditional.6 = ((f32[4,2,256]{2,1,0:T(2,128)S(1)}, f32[4,2,256]{2,1,0:T(2,128)S(1)})) conditional(s32[]{:T(128)} %convert_element_type.85, (f32[4,2,256]{2,1,0:T(2,128)S(1)}, f32[4,2,256]{2,1,0:T(2,128)S(1)}) %tuple.87, (s32[]{:T(128)}, s32[]{:T(128)}, bf16[2048,512]{0,1:T(8,128)(2,1)}, bf16[256,4,2,64]{0,3,2,1:T(8,128)(2,1)S(1)}, ...), branch_computations={%region_1.0_spmd, %region_2.4_spmd} | conditional | flops 142742272 | bytes 10730566 | solution.py:102
  149.3 3.2 %conditional.6 = ((f32[4,2,256]{2,1,0:T(2,128)S(1)}, f32[4,2,256]{2,1,0:T(2,128)S(1)})) conditional(s32[]{:T(128)} %convert_element_type.85, (f32[4,2,256]{2,1,0:T(2,128)S(1)}, f32[4,2,256]{2,1,0:T(2,128)S(1)}) %tuple.87, (s32[]{:T(128)}, s32[]{:T(128)}, bf16[2048,512]{0,1:T(8,128)(2,1)}, bf16[256,4,2,64]{0,3,2,1:T(8,128)(2,1)S(1)}, ...), branch_computations={%region_1.0_spmd, %region_2.4_spmd} | conditional | flops 142742272 | bytes 10730566 | solution.py:102
  152.5 3.2 %conditional.6 = ((f32[4,2,256]{2,1,0:T(2,128)S(1)}, f32[4,2,256]{2,1,0:T(2,128)S(1)})) conditional(s32[]{:T(128)} %convert_element_type.85, (f32[4,2,256]{2,1,0:T(2,128)S(1)}, f32[4,2,256]{2,1,0:T(2,128)S(1)}) %tuple.87, (s32[]{:T(128)}, s32[]{:T(128)}, bf16[2048,512]{0,1:T(8,128)(2,1)}, bf16[256,4,2,64]{0,3,2,1:T(8,128)(2,1)S(1)}, ...), branch_computations={%region_1.0_spmd, %region_2.4_spmd} | conditional | flops 142742272 | bytes 10730566 | solution.py:102
  155.8 3.2 %conditional.6 = ((f32[4,2,256]{2,1,0:T(2,128)S(1)}, f32[4,2,256]{2,1,0:T(2,128)S(1)})) conditional(s32[]{:T(128)} %convert_element_type.85, (f32[4,2,256]{2,1,0:T(2,128)S(1)}, f32[4,2,256]{2,1,0:T(2,128)S(1)}) %tuple.87, (s32[]{:T(128)}, s32[]{:T(128)}, bf16[2048,512]{0,1:T(8,128)(2,1)}, bf16[256,4,2,64]{0,3,2,1:T(8,128)(2,1)S(1)}, ...), branch_computations={%region_1.0_spmd, %region_2.4_spmd} | conditional | flops 142742272 | bytes 10730566 | solution.py:102
  159.0 44.9 %all-gather.6.cloned.1.call-done = bf16[2048,512]{0,1:T(8,128)(2,1)} async-done(((bf16[256,512]{0,1:T(8,128)(2,1)}), bf16[2048,512]{0,1:T(8,128)(2,1)}) %all-gather.6.cloned.1.call-update) | async-done | bytes 2097168 | tf_op jit(solution)/shard_map/all_gather | solution.py:108
  204.0 14.4 %while.34 = (s32[]{:T(128)}, f32[4,256,128]{2,1,0:T(8,128)S(1)}, s32[]{:T(128)}, bf16[2048,512]{0,1:T(8,128)(2,1)}, bf16[256,4,2,64]{0,3,2,1:T(8,128)(2,1)S(1)},...) while((s32[]{:T(128)}, f32[4,256,128]{2,1,0:T(8,128)S(1)}, ...), condition=%wide.region_9.10_spmd.clone, body=%wide.region_6.9_spmd.clone.sunk | while | flops 274465536 | bytes 13132077 | solution.py:132
  204.1 3.6 %conditional.7 = (f32[4,256,128]{2,1,0:T(8,128)S(1)}) conditional(s32[]{:T(128)} %convert_element_type.86, f32[4,256,128]{2,1,0:T(8,128)S(1)} %get-tuple-element.604, (s32[]{:T(128)}, s32[]{:T(128)}, bf16[2048,512]{0,1:T(8,128)(2,1)}, bf16[256,4,2,64]{0,3,2,1:T(8,128)(2,1)S(1)}, f32[4,2,256]{2,1,0:T(2,128)S(1)}, ...), branch_computations={%region_7.7_spmd, %region_8.8_spmd} | conditional | flops 274465536 | bytes 13130822 | solution.py:130
  207.6 3.6 %conditional.7 = (f32[4,256,128]{2,1,0:T(8,128)S(1)}) conditional(s32[]{:T(128)} %convert_element_type.86, f32[4,256,128]{2,1,0:T(8,128)S(1)} %get-tuple-element.604, (s32[]{:T(128)}, s32[]{:T(128)}, bf16[2048,512]{0,1:T(8,128)(2,1)}, bf16[256,4,2,64]{0,3,2,1:T(8,128)(2,1)S(1)}, f32[4,2,256]{2,1,0:T(2,128)S(1)}, ...), branch_computations={%region_7.7_spmd, %region_8.8_spmd} | conditional | flops 274465536 | bytes 13130822 | solution.py:130
  207.7 1.3 constant_dynamic-slice_fusion.1
  211.2 3.6 %conditional.7 = (f32[4,256,128]{2,1,0:T(8,128)S(1)}) conditional(s32[]{:T(128)} %convert_element_type.86, f32[4,256,128]{2,1,0:T(8,128)S(1)} %get-tuple-element.604, (s32[]{:T(128)}, s32[]{:T(128)}, bf16[2048,512]{0,1:T(8,128)(2,1)}, bf16[256,4,2,64]{0,3,2,1:T(8,128)(2,1)S(1)}, f32[4,2,256]{2,1,0:T(2,128)S(1)}, ...), branch_computations={%region_7.7_spmd, %region_8.8_spmd} | conditional | flops 274465536 | bytes 13130822 | solution.py:130
  211.3 1.3 constant_dynamic-slice_fusion.1
  214.8 3.6 %conditional.7 = (f32[4,256,128]{2,1,0:T(8,128)S(1)}) conditional(s32[]{:T(128)} %convert_element_type.86, f32[4,256,128]{2,1,0:T(8,128)S(1)} %get-tuple-element.604, (s32[]{:T(128)}, s32[]{:T(128)}, bf16[2048,512]{0,1:T(8,128)(2,1)}, bf16[256,4,2,64]{0,3,2,1:T(8,128)(2,1)S(1)}, f32[4,2,256]{2,1,0:T(2,128)S(1)}, ...), branch_computations={%region_7.7_spmd, %region_8.8_spmd} | conditional | flops 274465536 | bytes 13130822 | solution.py:130
  219.6 2.3 gather_fusion.1
  221.9 2.4 %reshape.127 = f32[128,2,2048]{2,1,0:T(2,128)S(1)} reshape(bf16[256,2048]{1,0:T(8,128)(2,1)} %gather_fusion.1) | data formatting | bytes 3145728 | tf_op jit(solution)/shard_map/convert_element_type | solution.py:176
  224.3 3.9 %multiply_reduce_fusion = bf16[128,2048]{1,0:T(8,128)(2,1)} fusion(f32[128,2,2048]{2,1,0:T(2,128)S(1)} %reshape.127, f32[128,2]{1,0:T(8,128)S(1)} %copy.44), kind=kLoop, calls=%fused_computation.28 | loop fusion | flops 786432 | bytes 2622464 | tf_op jit(solution)/shard_map/reduce_sum | solution.py:176
  (132 shorter events, 34.9 us)
Async XLA Ops:
  8.0 77.9 %copy-start = (bf16[1,256,2048]{2,1,0:T(8,128)(2,1)S(1)}, bf16[1,256,2048]{2,1,0:T(8,128)(2,1)}, u32[]{:S(2)}) copy-start(bf16[1,256,2048]{2,1,0:T(8,128)(2,1)} %param.33) | copy-start | bytes 3145732
  8.0 73.0 %all-gather.8.cloned.1.call-start = ((), (), s32[]{:S(2)}) async-start(), calls=%async_computation.5 | async-start | bytes 5242880 | tf_op jit(solution)/shard_map/all_gather | solution.py:154
  44.3 41.5 %copy-start.8 = (bf16[1,2048,256]{2,1,0:T(8,128)(2,1)S(1)}, bf16[1,2048,256]{2,1,0:T(8,128)(2,1)}, u32[]{:S(2)}) copy-start(bf16[1,2048,256]{2,1,0:T(8,128)(2,1)} %param.32) | copy-start | bytes 3145732
  44.4 94.5 %reduce-scatter.2.cloned.1.call-start = ((), (), s32[]{:S(2)}) async-start(), calls=%async_computation.6 | async-start | bytes 5242880 | tf_op jit(solution)/shard_map/reduce_scatter | solution.py:158
  94.6 0.9 copy-start.1
  94.6 1.9 copy-start.2
  94.6 2.7 %copy-start.3 = (bf16[256,512]{1,0:T(8,128)(2,1)S(1)}, bf16[256,512]{1,0:T(8,128)(2,1)}, u32[]{:S(2)}) copy-start(bf16[256,512]{1,0:T(8,128)(2,1)} %param.21) | copy-start | bytes 786436
  94.6 2.9 %copy-start.4 = (bf16[2048,8]{0,1:T(8,128)(2,1)S(1)}, bf16[2048,8]{0,1:T(8,128)(2,1)}, u32[]{:S(2)}) copy-start(bf16[2048,8]{0,1:T(8,128)(2,1)} %param.29) | copy-start | bytes 98308
  94.6 49.7 %copy-start.5 = (bf16[2048,4]{0,1:T(4,128)(2,1)S(1)}, bf16[2048,4]{0,1:T(4,128)(2,1)}, u32[]{:S(2)}) copy-start(bf16[2048,4]{0,1:T(4,128)(2,1)} %param.28) | copy-start | bytes 49156
  94.7 51.3 %all-gather.4.cloned.1.call-start = ((), (), s32[]{:S(2)}) async-start(), calls=%async_computation.3 | async-start | bytes 2359296 | tf_op jit(solution)/shard_map/all_gather | solution.py:107
  96.4 107.5 %all-gather.6.cloned.1.call-start = ((), (), s32[]{:S(2)}) async-start(), calls=%async_computation.4 | async-start | bytes 2359296 | tf_op jit(solution)/shard_map/all_gather | solution.py:108
  138.8 80.8 %all-to-all-start.1 = ((bf16[8,32,2048]{2,1,0:T(8,128)(2,1)}), bf16[8,32,2048]{2,1,0:T(8,128)(2,1)S(1)}, u32[]{:S(2)}, u32[]{:S(2)}) async-start(bf16[8,32,2048]{2,1,0:T(8,128)(2,1)} %bitcast.86), calls=%async_computation.2 | async-start | bytes 2097152 | tf_op jit(solution)/shard_map/all_to_all | solution.py:164
  146.0 58.0 %copy-start.6 = (f32[4]{0:T(128)S(1)}, f32[4]{0:T(128)}, u32[]{:S(2)}) copy-start(f32[4]{0:T(128)} %param.24) | copy-start | bytes 52
  204.0 14.6 %copy-start.7 = (f32[128]{0:T(128)S(1)}, f32[128]{0:T(128)}, u32[]{:S(2)}) copy-start(f32[128]{0:T(128)} %param.25) | copy-start | bytes 1540
Sparse Core Ops, SparseCore 0:
  44.5 36.4 all-gather.7
  94.8 43.9 reduce-scatter.1
Sparse Core Ops, SparseCore 1:
  97.8 48.2 all-gather.3
  148.5 55.4 all-gather.5
where the time goes:
time: 236 us
  waiting for transfers between devices  124 us (53%)
  blocking collectives  28.6 us (12%)
  matrix products  25.8 us (11%)
  local copies, waits for them, and re-layouts  20.7 us (9%)
  between operations  15.7 us (7%)
  other arithmetic  14.5 us (6%)
  starting transfers between devices  5.61 us (2%)
    all_gather x1, waiting for transfers between devices, local(): value_shard = lax.all_gather(values, 'ep', axis=0, tiled=True)  44.9 us
    reduce_scatter x1, waiting for transfers between devices, local(): lax.psum_scatter(jnp.dot(hidden, down_local, preferred_element_type=jnp.f...  41.1 us
    all_gather x1, waiting for transfers between devices, local(): lax.all_gather(arrived.reshape(-1, model_width), 'tp', axis=0, tiled=True)  36.6 us
    all_to_all x1, blocking collectives, local(): lax.all_to_all(packed, 'ep', split_axis=0, concat_axis=0, tiled=True)  28.6 us
    dot_general x1, matrix products, local(): jnp.dot(hidden, down_local, preferred_element_type=jnp.float32)  8.75 us
    dot_general x8, matrix products, score_block(): jnp.einsum('qhmd,khmd->hmqk', query_heads, key_heads, preferred_element_t...  8.44 us
    all_to_all x1, starting transfers between devices, local(): lax.all_to_all(summed.reshape(expert_count, capacity, model_width), 'ep',...  5.44 us
    dynamic_slice x4, local copies, waits for them, and re-layouts, value_compute(): lax.dynamic_slice_in_dim(value_shard, offset, value_block_rows, 0)  5.11 us
  transfers between devices with their start and end apart: 5, of which 4 were waited for; matrix products, arithmetic and copies ran while one was open for 13% of the time, Pallas kernels for 0%

commit v1 on v0

--- a/solution.py
+++ b/solution.py
@@ -104,8 +104,11 @@
     maxima, totals = lax.fori_loop(
         0, key_shard.shape[0] // block_rows, stats_sweep_step, stats_start
     )
-    value_key_shard = lax.all_gather(keys, "ep", axis=0, tiled=True)
-    value_shard = lax.all_gather(values, "ep", axis=0, tiled=True)
+    value_key_shard, value_shard = jnp.split(
+        lax.all_gather(jnp.concatenate([keys, values], axis=1), "ep", axis=0, tiled=True),
+        [keys.shape[1]],
+        axis=1,
+    )
     value_block_rows = math.gcd(value_key_shard.shape[0], 512)
 
     def value_sweep_step(number, current):

time: 236 us -> 268 us (1.14)
  waiting for transfers between devices: 124 us -> 150 us
  local copies, waits for them, and re-layouts: 20.7 us -> 24.8 us
    all_gather x2, waiting for transfers between devices: 46.1 us -> 73 us  [the longest x1 71.7 us: local(): lax.all_gather(jnp.concatenate([keys, values], axis=1), 'ep', axis=0, til...]
    split x0 -> x1, local copies, waits for them, and re-layouts: none -> 4.78 us  [local(): jnp.split(lax.all_gather(jnp.concatenate([keys, values], axis=1), 'ep', a...]
where the time goes in v1:
time: 268 us; the launch traced here: 267 us
  waiting for transfers between devices  150 us (56%)
  blocking collectives  28.6 us (11%)
  matrix products  25.8 us (10%)
  local copies, waits for them, and re-layouts  24.8 us (9%)
  other arithmetic  16.2 us (6%)
  between operations  15.7 us (6%)
  starting transfers between devices  5.61 us (2%)
    all_gather x1, waiting for transfers between devices, local(): lax.all_gather(jnp.concatenate([keys, values], axis=1), 'ep', axis=0, til...  71.7 us
    reduce_scatter x1, waiting for transfers between devices, local(): lax.psum_scatter(jnp.dot(hidden, down_local, preferred_element_type=jnp.f...  39.9 us
    all_gather x1, waiting for transfers between devices, local(): lax.all_gather(arrived.reshape(-1, model_width), 'tp', axis=0, tiled=True)  36.6 us
    all_to_all x1, blocking collectives, local(): lax.all_to_all(packed, 'ep', split_axis=0, concat_axis=0, tiled=True)  28.6 us
    dot_general x1, matrix products, local(): jnp.dot(hidden, down_local, preferred_element_type=jnp.float32)  8.8 us
    dot_general x8, matrix products, score_block(): jnp.einsum('qhmd,khmd->hmqk', query_heads, key_heads, preferred_element_t...  8.44 us
    all_to_all x1, starting transfers between devices, local(): lax.all_to_all(summed.reshape(expert_count, capacity, model_width), 'ep',...  5.44 us
  transfers between devices with their start and end apart: 5, of which 4 were waited for; matrix products, arithmetic and copies ran while one was open for 13% of the time, Pallas kernels for 0%

profile of v1, /device:TPU:25, one launch (start us, length us, event | category | flops | bytes accessed | tf_op | source)
XLA Modules:
  0.0 267.1 jit_solution(15566622941647486708)
XLA Ops:
  10.5 1.4 scatter_custom_fusion
  14.4 1.4 gather_fusion
  15.7 28.6 %all_to_all.10 = bf16[8,32,2048]{2,1,0:T(8,128)(2,1)} all-to-all(bf16[8,32,2048]{2,1,0:T(8,128)(2,1)S(1)} %bitcast.83), channel_id=1, replica_groups=mesh['ep'=8,'tp'=4] {'ep'}, dimensions={0} | all-to-all | bytes 2097152 | tf_op jit(solution)/shard_map/all_to_all | solution.py:156
  44.4 36.6 %all-gather.8.cloned.1.call-done = bf16[1024,2048]{1,0:T(8,128)(2,1)} async-done(((bf16[256,2048]{1,0:T(8,128)(2,1)}), bf16[1024,2048]{1,0:T(8,128)(2,1)}) %all-gather.8.cloned.1.call-update) | async-done | bytes 4194320 | tf_op jit(solution)/shard_map/all_gather | solution.py:157
  81.0 4.8 %fusion.18 = f32[1024,256]{1,0:T(8,128)} fusion(bf16[1024,2048]{1,0:T(8,128)(2,1)} %all-gather.8.cloned.1.call-done, bf16[1,2048,256]{2,1,0:T(8,128)(2,1)} %param.31), kind=kOutput, calls=%fused_computation.38 | convolution fusion | flops 1073741824 | bytes 6291456 | tf_op jit(solution)/shard_map/dot_general | solution.py:158
  85.8 8.8 %convolution_convert_fusion = bf16[1024,2048]{1,0:T(8,128)(2,1)} fusion(bf16[1024,2048]{1,0:T(8,128)(2,1)} %all-gather.8.cloned.1.call-done, bf16[1,256,2048]{2,1,0:T(8,128)(2,1)S(1)} %copy-done, bf16[1,2048,256]{2,1,0:T(8,128)(2,1)S(1)} %copy-done.8, f32[1024,256]{1,0:T(8,128)} %fusion.18), kind=kOutput, calls=%fused_computation.27 | convolution fusion | flops 2151153664 | bytes 11534336 | tf_op jit(solution)/shard_map/dot_general | solution.py:162
  96.7 1.8 pad_maximum_fusion
  99.0 39.9 %reduce-scatter.2.cloned.1.call-done = bf16[256,2048]{1,0:T(8,128)(2,1)} async-done(((bf16[1024,2048]{1,0:T(8,128)(2,1)}), bf16[256,2048]{1,0:T(8,128)(2,1)}) %reduce-scatter.2.cloned.1.call-update) | async-done | bytes 1048592 | tf_op jit(solution)/shard_map/reduce_scatter | solution.py:161
  138.9 5.4 %all-to-all-start.1 = ((bf16[8,32,2048]{2,1,0:T(8,128)(2,1)}), bf16[8,32,2048]{2,1,0:T(8,128)(2,1)S(1)}, u32[]{:S(2)}, u32[]{:S(2)}) async-start(bf16[8,32,2048]{2,1,0:T(8,128)(2,1)} %bitcast.86), calls=%async_computation.2 | async-start | bytes 2097152 | tf_op jit(solution)/shard_map/all_to_all | solution.py:167
  146.0 12.9 %while.33 = (s32[]{:T(128)}, f32[4,2,256]{2,1,0:T(2,128)S(1)}, f32[4,2,256]{2,1,0:T(2,128)S(1)}, s32[]{:T(128)}, bf16[2048,512]{0,1:T(8,128)(2,1)}, /*index=5*/b...) while((s32[]{:T(128)}, f32[4,2,256]{2,1,0:T(2,128)S(1)}, ...), condition=%wide.region_5.6_spmd.clone, body=%wide.region_0.5_spmd.clone.sunk | while | flops 142742272 | bytes 10731781 | solution.py:104
  146.0 3.2 %conditional.6 = ((f32[4,2,256]{2,1,0:T(2,128)S(1)}, f32[4,2,256]{2,1,0:T(2,128)S(1)})) conditional(s32[]{:T(128)} %convert_element_type.85, (f32[4,2,256]{2,1,0:T(2,128)S(1)}, f32[4,2,256]{2,1,0:T(2,128)S(1)}) %tuple.89, (s32[]{:T(128)}, s32[]{:T(128)}, bf16[2048,512]{0,1:T(8,128)(2,1)}, bf16[256,4,2,64]{0,3,2,1:T(8,128)(2,1)S(1)}, ...), branch_computations={%region_1.0_spmd, %region_2.4_spmd} | conditional | flops 142742272 | bytes 10730566 | solution.py:102
  149.3 3.2 %conditional.6 = ((f32[4,2,256]{2,1,0:T(2,128)S(1)}, f32[4,2,256]{2,1,0:T(2,128)S(1)})) conditional(s32[]{:T(128)} %convert_element_type.85, (f32[4,2,256]{2,1,0:T(2,128)S(1)}, f32[4,2,256]{2,1,0:T(2,128)S(1)}) %tuple.89, (s32[]{:T(128)}, s32[]{:T(128)}, bf16[2048,512]{0,1:T(8,128)(2,1)}, bf16[256,4,2,64]{0,3,2,1:T(8,128)(2,1)S(1)}, ...), branch_computations={%region_1.0_spmd, %region_2.4_spmd} | conditional | flops 142742272 | bytes 10730566 | solution.py:102
  152.5 3.2 %conditional.6 = ((f32[4,2,256]{2,1,0:T(2,128)S(1)}, f32[4,2,256]{2,1,0:T(2,128)S(1)})) conditional(s32[]{:T(128)} %convert_element_type.85, (f32[4,2,256]{2,1,0:T(2,128)S(1)}, f32[4,2,256]{2,1,0:T(2,128)S(1)}) %tuple.89, (s32[]{:T(128)}, s32[]{:T(128)}, bf16[2048,512]{0,1:T(8,128)(2,1)}, bf16[256,4,2,64]{0,3,2,1:T(8,128)(2,1)S(1)}, ...), branch_computations={%region_1.0_spmd, %region_2.4_spmd} | conditional | flops 142742272 | bytes 10730566 | solution.py:102
  155.8 3.2 %conditional.6 = ((f32[4,2,256]{2,1,0:T(2,128)S(1)}, f32[4,2,256]{2,1,0:T(2,128)S(1)})) conditional(s32[]{:T(128)} %convert_element_type.85, (f32[4,2,256]{2,1,0:T(2,128)S(1)}, f32[4,2,256]{2,1,0:T(2,128)S(1)}) %tuple.89, (s32[]{:T(128)}, s32[]{:T(128)}, bf16[2048,512]{0,1:T(8,128)(2,1)}, bf16[256,4,2,64]{0,3,2,1:T(8,128)(2,1)S(1)}, ...), branch_computations={%region_1.0_spmd, %region_2.4_spmd} | conditional | flops 142742272 | bytes 10730566 | solution.py:102
  159.0 71.7 %all-gather.4.cloned.1.call-done = bf16[2048,1024]{0,1:T(8,128)(2,1)} async-done(((bf16[256,1024]{0,1:T(8,128)(2,1)}), bf16[2048,1024]{0,1:T(8,128)(2,1)}) %all-gather.4.cloned.1.call-update) | async-done | bytes 4194320 | tf_op jit(solution)/shard_map/all_gather | solution.py:108
  230.7 4.8 %fusion.34 = (bf16[2048,512]{0,1:T(8,128)(2,1)}, bf16[2048,512]{0,1:T(8,128)(2,1)}) fusion(bf16[2048,1024]{0,1:T(8,128)(2,1)} %all-gather.4.cloned.1.call-done), kind=kLoop, calls=%fused_computation.85 | loop fusion | bytes 8388608 | tf_op jit(solution)/shard_map/split | solution.py:107
  235.5 14.4 %while.34 = (s32[]{:T(128)}, f32[4,256,128]{2,1,0:T(8,128)S(1)}, s32[]{:T(128)}, bf16[2048,512]{0,1:T(8,128)(2,1)}, bf16[256,4,2,64]{0,3,2,1:T(8,128)(2,1)S(1)},...) while((s32[]{:T(128)}, f32[4,256,128]{2,1,0:T(8,128)S(1)}, ...), condition=%wide.region_9.10_spmd.clone, body=%wide.region_6.9_spmd.clone.sunk | while | flops 274465536 | bytes 13132069 | solution.py:135
  235.5 3.6 %conditional.7 = (f32[4,256,128]{2,1,0:T(8,128)S(1)}) conditional(s32[]{:T(128)} %convert_element_type.86, f32[4,256,128]{2,1,0:T(8,128)S(1)} %get-tuple-element.616, (s32[]{:T(128)}, s32[]{:T(128)}, bf16[2048,512]{0,1:T(8,128)(2,1)}, bf16[256,4,2,64]{0,3,2,1:T(8,128)(2,1)S(1)}, f32[4,2,256]{2,1,0:T(2,128)S(1)}, ...), branch_computations={%region_7.7_spmd, %region_8.8_spmd} | conditional | flops 274465536 | bytes 13130822 | solution.py:133
  239.1 3.6 %conditional.7 = (f32[4,256,128]{2,1,0:T(8,128)S(1)}) conditional(s32[]{:T(128)} %convert_element_type.86, f32[4,256,128]{2,1,0:T(8,128)S(1)} %get-tuple-element.616, (s32[]{:T(128)}, s32[]{:T(128)}, bf16[2048,512]{0,1:T(8,128)(2,1)}, bf16[256,4,2,64]{0,3,2,1:T(8,128)(2,1)S(1)}, f32[4,2,256]{2,1,0:T(2,128)S(1)}, ...), branch_computations={%region_7.7_spmd, %region_8.8_spmd} | conditional | flops 274465536 | bytes 13130822 | solution.py:133
  242.7 3.6 %conditional.7 = (f32[4,256,128]{2,1,0:T(8,128)S(1)}) conditional(s32[]{:T(128)} %convert_element_type.86, f32[4,256,128]{2,1,0:T(8,128)S(1)} %get-tuple-element.616, (s32[]{:T(128)}, s32[]{:T(128)}, bf16[2048,512]{0,1:T(8,128)(2,1)}, bf16[256,4,2,64]{0,3,2,1:T(8,128)(2,1)S(1)}, f32[4,2,256]{2,1,0:T(2,128)S(1)}, ...), branch_computations={%region_7.7_spmd, %region_8.8_spmd} | conditional | flops 274465536 | bytes 13130822 | solution.py:133
  246.3 3.6 %conditional.7 = (f32[4,256,128]{2,1,0:T(8,128)S(1)}) conditional(s32[]{:T(128)} %convert_element_type.86, f32[4,256,128]{2,1,0:T(8,128)S(1)} %get-tuple-element.616, (s32[]{:T(128)}, s32[]{:T(128)}, bf16[2048,512]{0,1:T(8,128)(2,1)}, bf16[256,4,2,64]{0,3,2,1:T(8,128)(2,1)S(1)}, f32[4,2,256]{2,1,0:T(2,128)S(1)}, ...), branch_computations={%region_7.7_spmd, %region_8.8_spmd} | conditional | flops 274465536 | bytes 13130822 | solution.py:133
  251.0 2.3 gather_fusion.1
  253.4 2.4 reshape.127
  255.8 3.9 %multiply_reduce_fusion = bf16[128,2048]{1,0:T(8,128)(2,1)} fusion(f32[128,2,2048]{2,1,0:T(2,128)S(1)} %reshape.127, f32[128,2]{1,0:T(8,128)S(1)} %copy.47), kind=kLoop, calls=%fused_computation.28 | loop fusion | flops 786432 | bytes 2622464 | tf_op jit(solution)/shard_map/reduce_sum | solution.py:179
  (134 shorter events, 36.8 us)
Async XLA Ops:
  8.0 77.8 %copy-start = (bf16[1,256,2048]{2,1,0:T(8,128)(2,1)S(1)}, bf16[1,256,2048]{2,1,0:T(8,128)(2,1)}, u32[]{:S(2)}) copy-start(bf16[1,256,2048]{2,1,0:T(8,128)(2,1)} %param.33) | copy-start | bytes 3145732
  8.0 73.0 %all-gather.8.cloned.1.call-start = ((), (), s32[]{:S(2)}) async-start(), calls=%async_computation.5 | async-start | bytes 5242880 | tf_op jit(solution)/shard_map/all_gather | solution.py:157
  44.3 41.5 %copy-start.8 = (bf16[1,2048,256]{2,1,0:T(8,128)(2,1)S(1)}, bf16[1,2048,256]{2,1,0:T(8,128)(2,1)}, u32[]{:S(2)}) copy-start(bf16[1,2048,256]{2,1,0:T(8,128)(2,1)} %param.32) | copy-start | bytes 3145732
  44.4 94.5 %reduce-scatter.2.cloned.1.call-start = ((), (), s32[]{:S(2)}) async-start(), calls=%async_computation.6 | async-start | bytes 5242880 | tf_op jit(solution)/shard_map/reduce_scatter | solution.py:161
  94.6 0.9 copy-start.1
  94.6 1.9 copy-start.2
  94.6 3.8 %copy-start.4 = (bf16[2048,8]{0,1:T(8,128)(2,1)S(1)}, bf16[2048,8]{0,1:T(8,128)(2,1)}, u32[]{:S(2)}) copy-start(bf16[2048,8]{0,1:T(8,128)(2,1)} %param.29) | copy-start | bytes 98308
  94.7 4.1 %copy-start.5 = (bf16[2048,4]{0,1:T(4,128)(2,1)S(1)}, bf16[2048,4]{0,1:T(4,128)(2,1)}, u32[]{:S(2)}) copy-start(bf16[2048,4]{0,1:T(4,128)(2,1)} %param.28) | copy-start | bytes 49156
  94.7 49.9 %copy-start.3 = (bf16[256,512]{1,0:T(8,128)(2,1)S(1)}, bf16[256,512]{1,0:T(8,128)(2,1)}, u32[]{:S(2)}) copy-start(bf16[256,512]{1,0:T(8,128)(2,1)} %param.21) | copy-start | bytes 786436
  94.7 51.3 %all-gather.6.cloned.1.call-start = ((), (), s32[]{:S(2)}) async-start(), calls=%async_computation.4 | async-start | bytes 2359296 | tf_op jit(solution)/shard_map/all_gather | solution.py:84
  96.5 134.2 %all-gather.4.cloned.1.call-start = ((), (), s32[]{:S(2)}) async-start(), calls=%async_computation.3 | async-start | bytes 4718592 | tf_op jit(solution)/shard_map/all_gather | solution.py:108
  138.9 112.2 %all-to-all-start.1 = ((bf16[8,32,2048]{2,1,0:T(8,128)(2,1)}), bf16[8,32,2048]{2,1,0:T(8,128)(2,1)S(1)}, u32[]{:S(2)}, u32[]{:S(2)}) async-start(bf16[8,32,2048]{2,1,0:T(8,128)(2,1)} %bitcast.86), calls=%async_computation.2 | async-start | bytes 2097152 | tf_op jit(solution)/shard_map/all_to_all | solution.py:167
  159.0 76.5 %copy-start.6 = (f32[4]{0:T(128)S(1)}, f32[4]{0:T(128)}, u32[]{:S(2)}) copy-start(f32[4]{0:T(128)} %param.24) | copy-start | bytes 52
  235.5 14.6 %copy-start.7 = (f32[128]{0:T(128)S(1)}, f32[128]{0:T(128)}, u32[]{:S(2)}) copy-start(f32[128]{0:T(128)} %param.25) | copy-start | bytes 1540
Sparse Core Ops, SparseCore 0:
  44.5 36.4 all-gather.7
  94.8 44.0 reduce-scatter.1
Sparse Core Ops, SparseCore 1:
  97.8 48.2 all-gather.5
  148.5 82.1 all-gather.3
